TPU v7x, 32 devices: a whole 2x2x4 slice. The times are simulated.
32 devices in a mesh: grp: 2 (over x), tp: 16 (over z, y, core).
Axes of the slice: x: 2, y: 2, z: 4, core: 2. Of those that a mesh axis runs over, the one named last changes fastest.
Arguments:
- residual_channel: bfloat16 [256, 8, 4096], P('grp', None, 'tp'), parts along dimension 0, may hold values from -18 to 18, as said below
- prior_block_multiplier: float32 [2, 4096], replicated, may hold values from 0.1 to 1.9
- probe_map_matrix: bfloat16 [2, 4096, 2048], P(None, None, 'tp'), may hold values from -0.09375 to 0.09375
- lookup_map_matrix: bfloat16 [2, 4096, 2048], P(None, None, 'tp'), may hold values from -0.09375 to 0.09375
- content_map_matrix: bfloat16 [2, 4096, 2048], P(None, None, 'tp'), may hold values from -0.09375 to 0.09375
- emission_valve_matrix: bfloat16 [2, 4096, 2048], P(None, None, 'tp'), may hold values from -0.09375 to 0.09375
- forgetting_map_matrix: bfloat16 [2, 4096, 32], replicated, may hold values from -0.09375 to 0.09375
- insertion_rate_matrix: bfloat16 [2, 4096, 32], replicated, may hold values from -0.09375 to 0.09375
- forgetting_magnitude_exponent: float32 [2, 32], P(None, 'tp'), may hold values from -4.6 to -1.2
- channel_forgetting_offset: float32 [2, 32], P(None, 'tp'), may hold values from -2 to 1
- surplus_forgetting_amounts: float32 [2, 256, 8, 32], P(None, 'grp', None, 'tp'), parts along dimension 1, may hold values from -0.7 to 0
- readout_rescale_multiplier: float32 [2, 2048], P(None, 'tp'), may hold values from 0.1 to 1.9
- emission_map_matrix: bfloat16 [2, 2048, 4096], P(None, None, 'tp'), may hold values from -2 to 2
- post_mixing_multiplier: float32 [2, 4096], replicated, may hold values from 0.1 to 1.9
- recurrent_matrices: float32 [2, 256, 32, 4096], P(None, 'grp', 'tp'), parts along dimension 1, may hold values from -6 to 6
Outputs:
- new_stream: bfloat16 [256, 8, 4096], P('grp', None, 'tp'), parts along dimension 0
- new_memory: float32 [2, 256, 32, 4096], P(None, 'grp', 'tp'), parts along dimension 1
There are 2 independent parts, one for each index of `grp`. A program takes and returns all parts, laid end to end along the dimension named above; an argument that names none is the same for every part. Nothing has to cross between parts.
Inputs may be any that keep to these rules, and one draw needn't show every extreme that they name: `residual_channel`: column scales of the features differ widely.
All inputs are finite; a program needn't handle non-finite values.
Results may differ from a plain program's by a relative error of at most 0.0081.
Values may be sent and summed in bfloat16 or wider, within the bound.
A program may use at most 192 MiB of HBM per device.

v0:
```python
import jax
import jax.numpy as jnp
from jax import lax
from jax.sharding import PartitionSpec as P

D = 4096
HEAD_DIM = 64
LAYERS = 2
EPS = 1e-06
HIGH = lax.Precision.HIGHEST


def solve_lower(a_mat, right_side):
    length = right_side.shape[-2]
    solved_rows = []
    for row_at in range(length):
        current_row = right_side[..., row_at, :]
        for col_at in range(row_at):
            current_row = current_row - a_mat[..., row_at, col_at][..., None] * solved_rows[col_at]
        solved_rows.append(current_row)
    return jnp.stack(solved_rows, axis=-2)


def delta_block(queries, key_rows, values, forgetting_exponent_amount, strength, matrix_state):
    length = queries.shape[2]
    causal = jnp.tril(jnp.ones((length, length), bool))
    strict = jnp.tril(jnp.ones((length, length), bool), -1)
    cumulative = jnp.cumsum(forgetting_exponent_amount, axis=-1)
    decay_mat = jnp.where(
        causal,
        jnp.exp(jnp.where(causal, cumulative[..., :, None] - cumulative[..., None, :], 0.0)),
        0.0,
    )
    key_gram = jnp.einsum("bhtd,bhsd->bhts", key_rows, key_rows, precision=HIGH)
    a_mat = jnp.where(strict, strength[..., :, None] * decay_mat * key_gram, 0.0)
    right_side = jnp.concatenate(
        [strength[..., None] * values, (strength * jnp.exp(cumulative))[..., None] * key_rows],
        axis=-1,
    )
    solved = solve_lower(a_mat, right_side)
    width_v = values.shape[-1]
    update = solved[..., :width_v] - jnp.einsum(
        "bhtk,bhkv->bhtv", solved[..., width_v:], matrix_state, precision=HIGH
    )
    scores = jnp.einsum("bhtd,bhsd->bhts", queries, key_rows, precision=HIGH) * decay_mat
    output = jnp.exp(cumulative)[..., None] * jnp.einsum(
        "bhtk,bhkv->bhtv", queries, matrix_state, precision=HIGH
    )
    output = output + jnp.einsum("bhts,bhsv->bhtv", scores, update, precision=HIGH)
    final_log = cumulative[..., -1:]
    revised_memory_matrix = jnp.exp(final_log)[..., None] * matrix_state + jnp.einsum(
        "bhsk,bhsv->bhkv",
        key_rows * jnp.exp(final_log - cumulative)[..., None],
        update,
        precision=HIGH,
    )
    return (output, revised_memory_matrix)


def unit_rows(matrix):
    return matrix * lax.rsqrt(jnp.sum(matrix * matrix, axis=-1, keepdims=True) + EPS)


def token_blender(
    mapped_token_vectors,
    magnitude_exponent,
    offset_terms_array,
    surplus_forgetting_exponent,
    multiplier_terms_array,
    incoming_memory_matrix,
    batch_total,
    generation_round_total,
):
    rounded = [
        lax.optimization_barrier(part_sum.astype(jnp.bfloat16)).astype(jnp.float32)
        for part_sum in mapped_token_vectors
    ]
    queries, keys_raw, values_raw, gate_raw, decay_pre, strength_pre = rounded
    head_count = incoming_memory_matrix.shape[1]

    def to_heads(matrix):
        return matrix.reshape(batch_total, generation_round_total, head_count, HEAD_DIM).transpose(
            0, 2, 1, 3
        )

    def per_head(matrix):
        return matrix.reshape(batch_total, generation_round_total, head_count).transpose(0, 2, 1)

    queries = unit_rows(jax.nn.silu(to_heads(queries))) * HEAD_DIM ** (-0.5)
    key_rows = unit_rows(jax.nn.silu(to_heads(keys_raw)))
    values = jax.nn.silu(to_heads(values_raw))
    forgetting_exponent_amount = -jnp.exp(magnitude_exponent)[None, :, None] * jax.nn.softplus(
        per_head(decay_pre) + offset_terms_array[None, :, None]
    )
    forgetting_exponent_amount = forgetting_exponent_amount + surplus_forgetting_exponent.transpose(
        0, 2, 1
    )
    strength = jax.nn.sigmoid(per_head(strength_pre))
    matrix_state = incoming_memory_matrix.reshape(batch_total, head_count, HEAD_DIM, HEAD_DIM)
    output, revised_memory_matrix = delta_block(
        queries, key_rows, values, forgetting_exponent_amount, strength, matrix_state
    )
    normed = output * lax.rsqrt(jnp.mean(output * output, axis=-1, keepdims=True) + EPS)
    normed = (
        normed
        * multiplier_terms_array.reshape(head_count, HEAD_DIM)[None, :, None, :]
        * jax.nn.silu(to_heads(gate_raw))
    )
    blended_token_vectors = (
        normed.transpose(0, 2, 1, 3)
        .reshape(batch_total * generation_round_total, head_count * HEAD_DIM)
        .astype(jnp.bfloat16)
    )
    return (
        blended_token_vectors,
        revised_memory_matrix.reshape(batch_total, head_count, HEAD_DIM * HEAD_DIM),
    )


def project(portion, weights):
    return tuple(
        (jnp.dot(portion, weight, preferred_element_type=jnp.float32) for weight in weights)
    )


def out_project(blended_token_vectors, weight_rows):
    return jnp.dot(
        lax.all_gather(blended_token_vectors, "tp", axis=1, tiled=True),
        weight_rows,
        preferred_element_type=jnp.float32,
    ).astype(jnp.bfloat16)


def post_residual(widened, mixed_out, multiplier_terms_array, complete):
    mixed_wide = lax.optimization_barrier(mixed_out).astype(jnp.float32)
    squares = jnp.sum(mixed_wide * mixed_wide, axis=-1)
    if not complete:
        squares = lax.psum(squares, "tp")
    post_rms = lax.rsqrt(squares / D + EPS)[:, None]
    return lax.optimization_barrier(
        (widened + mixed_wide * post_rms * multiplier_terms_array).astype(jnp.bfloat16)
    )


def local(
    residual_channel,
    prior_block_multiplier,
    probe_map_matrix,
    lookup_map_matrix,
    content_map_matrix,
    emission_valve_matrix,
    forgetting_map_matrix,
    insertion_rate_matrix,
    forgetting_magnitude_exponent,
    channel_forgetting_offset,
    surplus_forgetting_amounts,
    readout_rescale_multiplier,
    emission_map_matrix,
    post_mixing_multiplier,
    recurrent_matrices,
):
    batch_total, generation_round_total, own_width = residual_channel.shape
    head_count = recurrent_matrices.shape[2]
    row_count = batch_total * generation_round_total
    col_offset = lax.axis_index("tp") * own_width
    head_offset = lax.axis_index("tp") * head_count
    new_states = []

    def mix_layer(mapped_token_vectors, block_index_number):
        blended_token_vectors, revised_memory_matrix = token_blender(
            mapped_token_vectors,
            forgetting_magnitude_exponent[block_index_number],
            channel_forgetting_offset[block_index_number],
            surplus_forgetting_amounts[block_index_number],
            readout_rescale_multiplier[block_index_number],
            recurrent_matrices[block_index_number],
            batch_total,
            generation_round_total,
        )
        new_states.append(revised_memory_matrix)
        return out_project(blended_token_vectors, emission_map_matrix[block_index_number])

    def own_cols(matrix):
        return lax.dynamic_slice_in_dim(matrix, col_offset, own_width, matrix.ndim - 1)

    whole_rows = lax.all_gather(
        residual_channel.reshape(row_count, own_width), "tp", axis=1, tiled=True
    )
    current = whole_rows
    for block_index_number in range(LAYERS):
        widened = whole_rows.astype(jnp.float32)
        inv_rms = lax.rsqrt(jnp.mean(widened * widened, axis=-1, keepdims=True) + EPS)
        hidden = (widened * inv_rms * prior_block_multiplier[block_index_number]).astype(
            jnp.bfloat16
        )
        weights = (
            probe_map_matrix[block_index_number],
            lookup_map_matrix[block_index_number],
            content_map_matrix[block_index_number],
            emission_valve_matrix[block_index_number],
            lax.dynamic_slice_in_dim(
                forgetting_map_matrix[block_index_number], head_offset, head_count, 1
            ),
            lax.dynamic_slice_in_dim(
                insertion_rate_matrix[block_index_number], head_offset, head_count, 1
            ),
        )
        mapped_token_vectors = project(hidden, weights)
        mixed_out = mix_layer(mapped_token_vectors, block_index_number)
        if block_index_number < LAYERS - 1:
            gathered = lax.all_gather(mixed_out, "tp", axis=1, tiled=True)
            whole_rows = post_residual(
                widened, gathered, post_mixing_multiplier[block_index_number], True
            )
        else:
            current = post_residual(
                own_cols(widened),
                mixed_out,
                own_cols(post_mixing_multiplier[block_index_number]),
                False,
            )
    return (
        current.reshape(batch_total, generation_round_total, own_width),
        jnp.stack(new_states, axis=0),
    )


def solution(mesh):
    return jax.shard_map(
        local,
        mesh=mesh,
        in_specs=(
            P("grp", None, "tp"),
            P(),
            P(None, None, "tp"),
            P(None, None, "tp"),
            P(None, None, "tp"),
            P(None, None, "tp"),
            P(),
            P(),
            P(None, "tp"),
            P(None, "tp"),
            P(None, "grp", None, "tp"),
            P(None, "tp"),
            P(None, None, "tp"),
            P(),
            P(None, "grp", "tp", None),
        ),
        out_specs=(P("grp", None, "tp"), P(None, "grp", "tp", None)),
        check_vma=False,
    )
```

profile of v0, /device:TPU:0, one launch (start us, length us, event | category | flops | bytes accessed | tf_op | source)
XLA Modules:
  0.0 673.6 jit_solution(834577331812609737)
XLA Ops:
  11.3 14.3 %fusion.190 = (f32[1,128,2,4096]{3,2,1,0:T(2,128)}, f32[1,128,2,4096]{3,2,1,0:T(2,128)}) fusion(f32[2,128,2,4096]{3,2,1,0:T(2,128)} %param.29), kind=kLoop, calls=%fused_computation.324 | loop fusion | bytes 16777216 | tf_op jit(solution)/shard_map/slice | solution.py:176
  25.6 7.4 %copy.607 = f32[1,128,2,4096]{1,3,2,0:T(8,128)} copy(f32[1,128,2,4096]{3,2,1,0:T(2,128)} %get-tuple-element.41) | data formatting | bytes 8388608
  33.1 9.3 %copy.482 = f32[128,2,64,64]{3,2,1,0:T(8,128)} copy(f32[128,2,64,64]{0,3,2,1:T(8,128)} %bitcast.322) | data formatting | bytes 8388608 | tf_op jit(solution)/shard_map/reshape;squeeze | solution.py:99
  44.6 46.0 %all-gather.5.cloned.1.call-done = bf16[1024,4096]{1,0:T(8,128)(2,1)} async-done(((bf16[1024,256]{1,0:T(8,128)(2,1)}), bf16[1024,4096]{1,0:T(8,128)(2,1)}) %all-gather.5.cloned.1.call-update) | async-done | bytes 8388624 | tf_op jit(solution)/shard_map/all_gather | solution.py:186
  95.7 10.5 %fusion.4 = bf16[1024,4096]{1,0:T(8,128)(2,1)} fusion(bf16[1024,4096]{1,0:T(8,128)(2,1)} %all-gather.5.cloned.1.call-done, f32[4096]{0:T(1024)S(1)} %bitcast.336, f32[1024]{0:T(1024)S(1)} %add_rsqrt_fusion.7), kind=kLoop, calls=%fused_computation.9 | loop fusion | flops 16777216 | bytes 16797696 | tf_op jit(solution)/shard_map/convert_element_type | solution.py:193
  211.4 7.5 %fusion.72 = f32[128,2,8,64]{3,2,1,0:T(8,128)S(1)} fusion(f32[128,2,64,64]{3,2,1,0:T(8,128)S(1)} %bitcast.315, f32[128,2,8,64]{3,0,2,1:T(8,128)S(1)} %multiply_multiply_fusion.1), kind=kOutput, calls=%fused_computation.126 | convolution fusion | flops 100663296 | bytes 5242880 | tf_op jit(solution)/shard_map/bhtk,bhkv->bhtv/dot_general | solution.py:46
  218.9 7.2 %fusion.46 = f32[128,2,8,64]{3,2,1,0:T(8,128)S(1)} fusion(f32[128,2,64,64]{3,2,1,0:T(8,128)S(1)} %bitcast.315, f32[128,2,8,64]{3,0,2,1:T(8,128)S(1)} %slice.467), kind=kOutput, calls=%fused_computation.90 | convolution fusion | flops 100663296 | bytes 5242880 | tf_op jit(solution)/shard_map/bhtk,bhkv->bhtv/dot_general | solution.py:42
  237.5 50.8 %all-gather.7.cloned.1.call-done = bf16[1024,2048]{1,0:T(8,128)(2,1)} async-done(((bf16[1024,128]{1,0:T(8,128)(2,1)}), bf16[1024,2048]{1,0:T(8,128)(2,1)}) %all-gather.7.cloned.1.call-update) | async-done | bytes 4194320 | tf_op jit(solution)/shard_map/all_gather | solution.py:128
  293.7 7.4 %copy.609 = f32[1,128,2,4096]{1,3,2,0:T(8,128)} copy(f32[1,128,2,4096]{3,2,1,0:T(2,128)} %get-tuple-element.40) | data formatting | bytes 8388608
  301.1 9.1 %copy.539 = f32[128,2,64,64]{3,2,1,0:T(8,128)} copy(f32[128,2,64,64]{0,3,2,1:T(8,128)} %bitcast.323) | data formatting | bytes 8388608 | tf_op jit(solution)/shard_map/reshape;squeeze | solution.py:99
  310.8 58.1 %all-gather.9.cloned.1.call-done = bf16[1024,4096]{1,0:T(8,128)(2,1)} async-done(((bf16[1024,256]{1,0:T(8,128)(2,1)}), bf16[1024,4096]{1,0:T(8,128)(2,1)}) %all-gather.9.cloned.1.call-update) | async-done | bytes 8388624 | tf_op jit(solution)/shard_map/all_gather | solution.py:211
  374.7 6.9 %fusion.5 = bf16[1024,4096]{1,0:T(8,128)(2,1)S(1)} fusion(bf16[1024,4096]{1,0:T(8,128)(2,1)S(1)} %copy-done.1, bf16[1024,4096]{1,0:T(8,128)(2,1)} %all-gather.5.cloned.1.call-done, f32[4096]{0:T(1024)S(1)} %bitcast.334, f32[1024]{0:T(1024)S(1)} %add_rsqrt_fusion.6), kind=kLoop, calls=%fused_computation.10 | loop fusion | flops 25165824 | bytes 25186304 | tf_op jit(solution)/shard_map/convert_element_type | solution.py:141
  386.6 10.4 %multiply_convert_fusion = bf16[1024,4096]{1,0:T(8,128)(2,1)} fusion(f32[4096]{0:T(1024)S(1)} %bitcast.335, f32[1024]{0:T(1024)S(1)} %add_rsqrt_fusion.5, bf16[1024,4096]{1,0:T(8,128)(2,1)} %copy-done), kind=kLoop, calls=%fused_computation.11 | loop fusion | flops 16777216 | bytes 16797696 | tf_op jit(solution)/shard_map/convert_element_type | solution.py:193
  411.2 6.8 %convolution_convert_fusion.2 = bf16[1024,128]{1,0:T(8,128)(2,1)} fusion(bf16[1024,4096]{1,0:T(8,128)(2,1)} %multiply_convert_fusion, bf16[2,4096,128]{2,1,0:T(8,128)(2,1)} %param.20), kind=kOutput, calls=%fused_computation.26 | convolution fusion | flops 1073872896 | bytes 9699328 | tf_op jit(solution)/shard_map/dot_general | solution.py:122
  464.3 10.4 %fusion.64 = f32[128,2,8,64]{3,2,1,0:T(8,128)} fusion(f32[128,2,64,64]{3,2,1,0:T(8,128)} %copy.539, f32[128,2,8,64]{3,0,2,1:T(8,128)S(1)} %copy-done.9), kind=kOutput, calls=%fused_computation.118 | convolution fusion | flops 100663296 | bytes 5242880 | tf_op jit(solution)/shard_map/bhtk,bhkv->bhtv/dot_general | solution.py:46
  523.9 7.2 %fusion.44 = f32[128,2,8,64]{3,2,1,0:T(8,128)S(1)} fusion(f32[128,2,64,64]{3,2,1,0:T(8,128)S(1)} %bitcast.317, f32[128,2,8,64]{3,0,2,1:T(8,128)S(1)} %slice.511), kind=kOutput, calls=%fused_computation.88 | convolution fusion | flops 100663296 | bytes 5242880 | tf_op jit(solution)/shard_map/bhtk,bhkv->bhtv/dot_general | solution.py:42
  543.0 18.4 %multiply_add_fusion.1 = f32[128,2,64,64]{3,2,1,0:T(8,128)} fusion(f32[128,2,64,64]{3,2,1,0:T(8,128)} %copy.482, f32[128,2]{1,0:T(8,128)S(1)} %bitcast.332, f32[128,2,8,64]{3,0,2,1:T(8,128)S(1)} %get-tuple-element.12, f32[128,2,8,64]{3,0,2,1:T(8,128)S(1)} %slice_subtract_fusion.1), kind=kOutput, calls=%fused_computation.15 | convolution fusion | flops 102760448 | bytes 9438208 | tf_op jit(solution)/shard_map/bhsk,bhsv->bhkv/dot_general | solution.py:51
  561.4 8.0 %copy.596 = f32[128,2,64,64]{0,3,2,1:T(8,128)} copy(f32[128,2,64,64]{3,2,1,0:T(8,128)} %multiply_add_fusion.1) | data formatting | bytes 8388608 | tf_op jit(solution)/shard_map/add | solution.py:51
  569.4 11.6 %convert_element_type.108 = f32[1024,4096]{1,0:T(8,128)} convert(bf16[1024,4096]{1,0:T(8,128)(2,1)} %copy-done) | non-fusion elementwise | flops 4194304 | bytes 25165824 | tf_op jit(solution)/shard_map/convert_element_type | solution.py:191
  582.0 18.6 %multiply_add_fusion = f32[128,2,64,64]{3,2,1,0:T(8,128)} fusion(f32[128,2,64,64]{3,2,1,0:T(8,128)} %copy.539, f32[128,2]{1,0:T(8,128)S(1)} %bitcast.333, f32[128,2,8,64]{3,0,2,1:T(8,128)S(1)} %copy-done.2, f32[128,2,8,64]{3,0,2,1:T(8,128)S(1)} %copy-done.4), kind=kOutput, calls=%fused_computation.14 | convolution fusion | flops 102760448 | bytes 9438208 | tf_op jit(solution)/shard_map/bhsk,bhsv->bhkv/dot_general | solution.py:51
  600.6 8.0 %copy.602 = f32[128,2,64,64]{0,3,2,1:T(8,128)} copy(f32[128,2,64,64]{3,2,1,0:T(8,128)} %multiply_add_fusion) | data formatting | bytes 8388608 | tf_op jit(solution)/shard_map/add | solution.py:51
  608.6 7.4 %pad_maximum_fusion = f32[2,128,2,4096]{1,3,2,0:T(8,128)} fusion(f32[1,128,2,4096]{1,3,2,0:T(8,128)} %bitcast.325, f32[1,128,2,4096]{1,3,2,0:T(8,128)} %bitcast.324), kind=kLoop, calls=%fused_computation.13 | loop fusion | flops 2097152 | bytes 16777216 | tf_op jit(solution)/shard_map/stack | solution.py:224
  616.0 13.3 %copy.603 = f32[2,128,2,4096]{3,2,1,0:T(2,128)} copy(f32[2,128,2,4096]{1,3,2,0:T(8,128)} %pad_maximum_fusion) | data formatting | bytes 16777216
  632.9 31.4 %psum.7 = f32[1024]{0:T(1024)S(1)} all-reduce(f32[1024]{0:T(1024)S(1)} %fusion.8), channel_id=1, replica_groups=mesh['grp'=2,'tp'=16] {'tp'}, use_global_device_ids=true, to_apply=%region_12.13 | all-reduce | flops 1024 | bytes 8192 | tf_op jit(solution)/shard_map/psum | solution.py:138
  (401 shorter events, 271.6 us)
Async XLA Ops:
  7.2 83.5 %all-gather.5.cloned.1.call-start = ((), (), s32[]{:S(2)}) async-start(), calls=%async_computation | async-start | bytes 8912896 | tf_op jit(solution)/shard_map/all_gather | solution.py:186
  7.9 280.4 %all-gather.7.cloned.1.call-start = ((), (), s32[]{:S(2)}) async-start(), calls=%async_computation.1 | async-start | bytes 4456448 | tf_op jit(solution)/shard_map/all_gather | solution.py:128
  33.1 10.8 %copy-start.13 = (bf16[2,4096,32]{1,2,0:T(8,128)(2,1)S(1)}, bf16[2,4096,32]{1,2,0:T(8,128)(2,1)}, u32[]{:S(2)}) copy-start(bf16[2,4096,32]{1,2,0:T(8,128)(2,1)} %param.22) | copy-start | bytes 1572868
  42.5 85.7 %copy-start.76 = (pred[8,8]{1,0:T(8,128)(4,1)}, pred[8,8]{1,0:T(8,128)(4,1)S(1)}, u32[]{:S(2)}) copy-start(pred[8,8]{1,0:T(8,128)(4,1)S(1)} %get-tuple-element.131) | copy-start | bytes 196
  42.5 85.7 %copy-start.77 = (pred[8,8]{1,0:T(8,128)(4,1)}, pred[8,8]{1,0:T(8,128)(4,1)S(1)}, u32[]{:S(2)}) copy-start(pred[8,8]{1,0:T(8,128)(4,1)S(1)} %get-tuple-element.130) | copy-start | bytes 196
  127.5 12.8 %slice-start.4 = ((s8[8388608]{0:T(1024)(128)(4,1)}), s8[4194304]{0:T(1024)(128)(4,1)S(1)}, s32[]{:S(2)}) async-start(s8[8388608]{0:T(1024)(128)(4,1)} %bitcast.318), calls=%async_computation.8 | async-start | bytes 8388608
  129.2 11.2 %slice-start.5 = ((s8[8388608]{0:T(1024)(128)(4,1)}), s8[4194304]{0:T(1024)(128)(4,1)S(1)}, s32[]{:S(2)}) async-start(s8[8388608]{0:T(1024)(128)(4,1)} %bitcast.318), calls=%async_computation.9 | async-start | bytes 8388608
  129.2 11.2 %copy-start.81 = (bf16[2,4096,128]{2,1,0:T(8,128)(2,1)S(1)}, bf16[2,4096,128]{2,1,0:T(8,128)(2,1)}, u32[]{:S(2)}) copy-start(bf16[2,4096,128]{2,1,0:T(8,128)(2,1)} %param.20) | copy-start | bytes 6291460
  232.8 60.1 %copy-start.80 = (f32[128]{0:T(128)S(1)}, f32[128]{0:T(128)}, u32[]{:S(2)}) copy-start(f32[128]{0:T(128)} %get-tuple-element.10) | copy-start | bytes 1540
  232.8 60.7 %copy-start.26 = (f32[1,128,8,2]{1,3,2,0:T(2,128)S(1)}, f32[1,128,8,2]{1,3,2,0:T(2,128)}, u32[]{:S(2)}) copy-start(f32[1,128,8,2]{1,3,2,0:T(2,128)} %get-tuple-element.119) | copy-start | bytes 24580
  237.5 131.4 %all-gather.9.cloned.1.call-start = ((), (), s32[]{:S(2)}) async-start(), calls=%async_computation.2 | async-start | bytes 8912896 | tf_op jit(solution)/shard_map/all_gather | solution.py:211
  292.9 336.4 %all-gather.11.cloned.1.call-start = ((), (), s32[]{:S(2)}) async-start(), calls=%async_computation.3 | async-start | bytes 4456448 | tf_op jit(solution)/shard_map/all_gather | solution.py:128
  397.1 12.4 %copy-start.73 = (f32[2]{0:T(128)S(1)}, f32[2]{0:T(128)}, u32[]{:S(2)}) copy-start(f32[2]{0:T(128)} %get-tuple-element.122) | copy-start | bytes 28
  397.1 12.4 %copy-start.74 = (f32[2]{0:T(128)S(1)}, f32[2]{0:T(128)}, u32[]{:S(2)}) copy-start(f32[2]{0:T(128)} %get-tuple-element.129) | copy-start | bytes 28
  410.5 23.3 %copy-start.21 = (f32[128,2,8]{2,1,0:T(2,128)}, f32[128,2,8]{2,1,0:T(2,128)S(1)}, u32[]{:S(2)}) copy-start(f32[128,2,8]{2,1,0:T(2,128)S(1)} %copy.544) | copy-start | bytes 24580
  411.2 13.4 %slice-start.6 = ((s8[8388608]{0:T(1024)(128)(4,1)}), s8[4194304]{0:T(1024)(128)(4,1)S(1)}, s32[]{:S(2)}) async-start(s8[8388608]{0:T(1024)(128)(4,1)} %bitcast.320), calls=%async_computation.10 | async-start | bytes 8388608
  434.7 11.7 %copy-start.18 = (f32[128,8,2]{1,0,2:T(8,128)S(1)}, f32[128,8,2]{1,0,2:T(8,128)}, u32[]{:S(2)}) copy-start(f32[128,8,2]{1,0,2:T(8,128)} %get-tuple-element.106) | copy-start | bytes 24580
  434.7 11.7 %copy-start.17 = (f32[128,2,8]{2,0,1:T(8,128)S(1)}, f32[128,2,8]{2,0,1:T(8,128)}, u32[]{:S(2)}) copy-start(f32[128,2,8]{2,0,1:T(8,128)} %get-tuple-element.107) | copy-start | bytes 24580
  434.7 12.4 %copy-start.16 = (f32[128,2,8]{2,0,1:T(8,128)S(1)}, f32[128,2,8]{2,0,1:T(8,128)}, u32[]{:S(2)}) copy-start(f32[128,2,8]{2,0,1:T(8,128)} %get-tuple-element.109) | copy-start | bytes 24580
  531.1 11.0 %copy-start.14 = (f32[128,2,1]{2,0,1:T(8,128)S(1)}, f32[128,2,1]{2,0,1:T(8,128)}, u32[]{:S(2)}) copy-start(f32[128,2,1]{2,0,1:T(8,128)} %get-tuple-element.102) | copy-start | bytes 3076
  569.4 11.7 %copy-start.15 = (f32[128,2,1]{2,0,1:T(8,128)S(1)}, f32[128,2,1]{2,0,1:T(8,128)}, u32[]{:S(2)}) copy-start(f32[128,2,1]{2,0,1:T(8,128)} %get-tuple-element.104) | copy-start | bytes 3076
  569.4 12.5 %copy-start.2 = (f32[128,2,8,64]{3,0,2,1:T(8,128)S(1)}, f32[128,2,8,64]{3,0,2,1:T(8,128)}, u32[]{:S(2)}) copy-start(f32[128,2,8,64]{3,0,2,1:T(8,128)} %get-tuple-element.14) | copy-start | bytes 1572868
  569.4 12.5 %copy-start.4 = (f32[128,2,8,64]{3,0,2,1:T(8,128)S(1)}, f32[128,2,8,64]{3,0,2,1:T(8,128)}, u32[]{:S(2)}) copy-start(f32[128,2,8,64]{3,0,2,1:T(8,128)} %copy-done.3) | copy-start | bytes 1572868
  616.0 13.3 %copy-start.87 = (bf16[2,2048,256]{2,1,0:T(8,128)(2,1)S(1)}, bf16[2,2048,256]{2,1,0:T(8,128)(2,1)}, u32[]{:S(2)}) copy-start(bf16[2,2048,256]{2,1,0:T(8,128)(2,1)} %param.27) | copy-start | bytes 6291460
  (77 other events, 356.0 us)
Sparse Core Ops, SparseCore 0:
  10.1 80.4 all-gather.4
  237.6 50.6 all-gather.6
  293.0 75.8 all-gather.8
  541.6 50.6 all-gather.10
where the time goes:
time: 680 us; the launch traced here: 674 us
  local copies, waits for them, and re-layouts  224 us (33%)
  matrix products  159 us (23%)
  waiting for transfers between devices  156 us (23%)
  other arithmetic  87.2 us (13%)
  blocking collectives  31.4 us (5%)
  between operations  15.9 us (2%)
    slice x60, local copies, waits for them, and re-layouts, solve_lower(): a_mat[..., row_at, col_at][..., None] * solved_rows[col_at]  95.2 us
    all_gather x1, waiting for transfers between devices, local(): gathered = lax.all_gather(mixed_out, 'tp', axis=1, tiled=True)  58.1 us
    dot_general x12, matrix products, project(): jnp.dot(portion, weight, preferred_element_type=jnp.float32)  55.6 us
    all_gather x2, waiting for transfers between devices, out_project(): lax.all_gather(blended_token_vectors, 'tp', axis=1, tiled=True)  50.8 us
    all_gather x1, waiting for transfers between devices, local(): lax.all_gather(residual_channel.reshape(row_count, own_width), 'tp', axis...  46 us
    unnamed x199, local copies, waits for them, and re-layouts  38.2 us
    dot_general x2, matrix products, delta_block(): jnp.einsum('bhsk,bhsv->bhkv', key_rows * jnp.exp(final_log - cumulative)[...  37 us
    psum x1, blocking collectives, post_residual(): squares = lax.psum(squares, 'tp')  31.4 us
  transfers between devices with their start and end apart: 4, of which 3 were waited for; matrix products, arithmetic and copies ran while one was open for 21% of the time, Pallas kernels for 0%

commit v1 on v0

--- a/solution.py
+++ b/solution.py
@@ -8,6 +8,17 @@
 LAYERS = 2
 EPS = 1e-06
 HIGH = lax.Precision.HIGHEST
+
+
+def turned_line(value, axis, along):
+    size = lax.axis_size(axis)
+    right = [(i, (i + 1) % size) for i in range(size)]
+    terms = [value]
+    for reach in range(1, size):
+        terms = [lax.ppermute(terms[0], axis, right), *terms]
+    result = jnp.concatenate(terms, axis=along)
+    turn = (lax.axis_index(axis) + 1) * terms[-1].shape[along]
+    return jnp.roll(result, turn, axis=along)
 
 
 def solve_lower(a_mat, right_side):
@@ -208,7 +219,7 @@
         mapped_token_vectors = project(hidden, weights)
         mixed_out = mix_layer(mapped_token_vectors, block_index_number)
         if block_index_number < LAYERS - 1:
-            gathered = lax.all_gather(mixed_out, "tp", axis=1, tiled=True)
+            gathered = turned_line(mixed_out, "tp", 1)
             whole_rows = post_residual(
                 widened, gathered, post_mixing_multiplier[block_index_number], True
             )

time: 680 us -> 810 us (1.19)
  waiting for transfers between devices: 156 us -> 251 us
  local copies, waits for them, and re-layouts: 224 us -> 285 us
  other arithmetic: 87.2 us -> 68.4 us
  matrix products: 159 us -> 149 us
    ppermute x0 -> x15, waiting for transfers between devices: none -> 158 us  [turned_line(): terms = [lax.ppermute(terms[0], axis, right), *terms]]
    all_gather x1 -> x0, waiting for transfers between devices: 58.1 us -> none  [local(): gathered = lax.all_gather(mixed_out, 'tp', axis=1, tiled=True)]
    unnamed x199 -> x280, local copies, waits for them, and re-layouts: 38.2 us -> 86.6 us
    convert_element_type x2, other arithmetic: 21 us -> 4.25 us  [local(): (widened * inv_rms * prior_block_multiplier[block_index_number]).astype(j...]
    dot_general x12, matrix products: 55.6 us -> 45.9 us  [project(): jnp.dot(portion, weight, preferred_element_type=jnp.float32)]
  transfers between devices with their start and end apart: 4 -> 18, of which waited for: 3 -> 16; matrix products, arithmetic and copies ran while one was open for 21% -> 18% of each run, Pallas kernels for 0% -> 0%
where the time goes in v1:
time: 810 us; the launch traced here: 799 us
  local copies, waits for them, and re-layouts  285 us (35%)
  waiting for transfers between devices  251 us (31%)
  matrix products  149 us (18%)
  other arithmetic  68.4 us (8%)
  blocking collectives  29.5 us (4%)
  between operations  16 us (2%)
    ppermute x15, waiting for transfers between devices, turned_line(): terms = [lax.ppermute(terms[0], axis, right), *terms]  158 us
    slice x60, local copies, waits for them, and re-layouts, solve_lower(): a_mat[..., row_at, col_at][..., None] * solved_rows[col_at]  95.4 us
    unnamed x280, local copies, waits for them, and re-layouts  86.6 us
    all_gather x2, waiting for transfers between devices, out_project(): lax.all_gather(blended_token_vectors, 'tp', axis=1, tiled=True)  51.2 us
    dot_general x12, matrix products, project(): jnp.dot(portion, weight, preferred_element_type=jnp.float32)  45.9 us
    all_gather x1, waiting for transfers between devices, local(): lax.all_gather(residual_channel.reshape(row_count, own_width), 'tp', axis...  41.9 us
    dot_general x2, matrix products, delta_block(): jnp.einsum('bhsk,bhsv->bhkv', key_rows * jnp.exp(final_log - cumulative)[...  36.8 us
    psum x1, blocking collectives, post_residual(): squares = lax.psum(squares, 'tp')  29.5 us
  transfers between devices with their start and end apart: 18, of which 16 were waited for; matrix products, arithmetic and copies ran while one was open for 18% of the time, Pallas kernels for 0%

profile of v1, /device:TPU:0, one launch (start us, length us, event | category | flops | bytes accessed | tf_op | source)
XLA Modules:
  0.0 798.7 jit_solution(11706103741222676552)
XLA Ops:
  12.8 14.3 %fusion.190 = (f32[1,128,2,4096]{3,2,1,0:T(2,128)}, f32[1,128,2,4096]{3,2,1,0:T(2,128)}) fusion(f32[2,128,2,4096]{3,2,1,0:T(2,128)} %param.29), kind=kLoop, calls=%fused_computation.357 | loop fusion | bytes 16777216 | tf_op jit(solution)/shard_map/slice | solution.py:187
  34.4 9.3 %copy.495 = f32[128,2,64,64]{3,2,1,0:T(8,128)} copy(f32[128,2,64,64]{0,3,2,1:T(8,128)} %bitcast.322) | data formatting | bytes 8388608 | tf_op jit(solution)/shard_map/reshape;squeeze | solution.py:110
  45.9 41.9 %all-gather.4.cloned.1.call-done = bf16[1024,4096]{0,1:T(8,128)(2,1)} async-done(((bf16[1024,256]{0,1:T(8,128)(2,1)}), bf16[1024,4096]{0,1:T(8,128)(2,1)}) %all-gather.4.cloned.1.call-update) | async-done | bytes 8388624 | tf_op jit(solution)/shard_map/all_gather | solution.py:197
  225.3 51.2 %all-gather.6.cloned.1.call-done = bf16[1024,2048]{1,0:T(8,128)(2,1)} async-done(((bf16[1024,128]{1,0:T(8,128)(2,1)}), bf16[1024,2048]{1,0:T(8,128)(2,1)}) %all-gather.6.cloned.1.call-update) | async-done | bytes 4194320 | tf_op jit(solution)/shard_map/all_gather | solution.py:139
  280.5 11.1 %collective-permute-done = bf16[1024,256]{0,1:T(8,128)(2,1)S(1)} collective-permute-done((bf16[1024,256]{0,1:T(8,128)(2,1)S(1)}, bf16[1024,256]{0,1:T(8,128)(2,1)S(1)}, u32[]{:S(2)}, u32[]{:S(2)}) %collective-permute-start) | collective-permute-done | bytes 524320 | tf_op jit(solution)/shard_map/ppermute | solution.py:18
  291.6 11.3 %collective-permute-done.1 = bf16[1024,256]{0,1:T(8,128)(2,1)S(1)} collective-permute-done((bf16[1024,256]{0,1:T(8,128)(2,1)S(1)}, bf16[1024,256]{0,1:T(8,128)(2,1)S(1)}, u32[]{:S(2)}, u32[]{:S(2)}) %collective-permute-start.1) | collective-permute-done | bytes 524320 | tf_op jit(solution)/shard_map/ppermute | solution.py:18
  303.7 11.3 %collective-permute-done.2 = bf16[1024,256]{0,1:T(8,128)(2,1)S(1)} collective-permute-done((bf16[1024,256]{0,1:T(8,128)(2,1)S(1)}, bf16[1024,256]{0,1:T(8,128)(2,1)S(1)}, u32[]{:S(2)}, u32[]{:S(2)}) %collective-permute-start.2) | collective-permute-done | bytes 524320 | tf_op jit(solution)/shard_map/ppermute | solution.py:18
  315.8 11.3 %collective-permute-done.3 = bf16[1024,256]{0,1:T(8,128)(2,1)S(1)} collective-permute-done((bf16[1024,256]{0,1:T(8,128)(2,1)S(1)}, bf16[1024,256]{0,1:T(8,128)(2,1)S(1)}, u32[]{:S(2)}, u32[]{:S(2)}) %collective-permute-start.3) | collective-permute-done | bytes 524320 | tf_op jit(solution)/shard_map/ppermute | solution.py:18
  327.9 11.3 %collective-permute-done.4 = bf16[1024,256]{0,1:T(8,128)(2,1)S(1)} collective-permute-done((bf16[1024,256]{0,1:T(8,128)(2,1)S(1)}, bf16[1024,256]{0,1:T(8,128)(2,1)S(1)}, u32[]{:S(2)}, u32[]{:S(2)}) %collective-permute-start.4) | collective-permute-done | bytes 524320 | tf_op jit(solution)/shard_map/ppermute | solution.py:18
  340.0 11.3 %collective-permute-done.5 = bf16[1024,256]{0,1:T(8,128)(2,1)S(1)} collective-permute-done((bf16[1024,256]{0,1:T(8,128)(2,1)S(1)}, bf16[1024,256]{0,1:T(8,128)(2,1)S(1)}, u32[]{:S(2)}, u32[]{:S(2)}) %collective-permute-start.5) | collective-permute-done | bytes 524320 | tf_op jit(solution)/shard_map/ppermute | solution.py:18
  352.1 11.3 %collective-permute-done.6 = bf16[1024,256]{0,1:T(8,128)(2,1)S(1)} collective-permute-done((bf16[1024,256]{0,1:T(8,128)(2,1)S(1)}, bf16[1024,256]{0,1:T(8,128)(2,1)S(1)}, u32[]{:S(2)}, u32[]{:S(2)}) %collective-permute-start.6) | collective-permute-done | bytes 524320 | tf_op jit(solution)/shard_map/ppermute | solution.py:18
  364.2 11.3 %collective-permute-done.7 = bf16[1024,256]{0,1:T(8,128)(2,1)S(1)} collective-permute-done((bf16[1024,256]{0,1:T(8,128)(2,1)S(1)}, bf16[1024,256]{0,1:T(8,128)(2,1)S(1)}, u32[]{:S(2)}, u32[]{:S(2)}) %collective-permute-start.7) | collective-permute-done | bytes 524320 | tf_op jit(solution)/shard_map/ppermute | solution.py:18
  376.3 11.3 %collective-permute-done.8 = bf16[1024,256]{0,1:T(8,128)(2,1)S(1)} collective-permute-done((bf16[1024,256]{0,1:T(8,128)(2,1)S(1)}, bf16[1024,256]{0,1:T(8,128)(2,1)S(1)}, u32[]{:S(2)}, u32[]{:S(2)}) %collective-permute-start.8) | collective-permute-done | bytes 524320 | tf_op jit(solution)/shard_map/ppermute | solution.py:18
  388.4 11.3 %collective-permute-done.9 = bf16[1024,256]{0,1:T(8,128)(2,1)S(1)} collective-permute-done((bf16[1024,256]{0,1:T(8,128)(2,1)S(1)}, bf16[1024,256]{0,1:T(8,128)(2,1)S(1)}, u32[]{:S(2)}, u32[]{:S(2)}) %collective-permute-start.9) | collective-permute-done | bytes 524320 | tf_op jit(solution)/shard_map/ppermute | solution.py:18
  400.5 11.3 %collective-permute-done.10 = bf16[1024,256]{0,1:T(8,128)(2,1)S(1)} collective-permute-done((bf16[1024,256]{0,1:T(8,128)(2,1)S(1)}, bf16[1024,256]{0,1:T(8,128)(2,1)S(1)}, u32[]{:S(2)}, u32[]{:S(2)}) %collective-permute-start.10) | collective-permute-done | bytes 524320 | tf_op jit(solution)/shard_map/ppermute | solution.py:18
  412.7 11.3 %collective-permute-done.11 = bf16[1024,256]{0,1:T(8,128)(2,1)S(1)} collective-permute-done((bf16[1024,256]{0,1:T(8,128)(2,1)S(1)}, bf16[1024,256]{0,1:T(8,128)(2,1)S(1)}, u32[]{:S(2)}, u32[]{:S(2)}) %collective-permute-start.11) | collective-permute-done | bytes 524320 | tf_op jit(solution)/shard_map/ppermute | solution.py:18
  424.7 11.4 %collective-permute-done.12 = bf16[1024,256]{0,1:T(8,128)(2,1)} collective-permute-done((bf16[1024,256]{0,1:T(8,128)(2,1)S(1)}, bf16[1024,256]{0,1:T(8,128)(2,1)}, u32[]{:S(2)}, u32[]{:S(2)}) %collective-permute-start.12) | collective-permute-done | bytes 524320 | tf_op jit(solution)/shard_map/ppermute | solution.py:18
  454.1 10.9 %collective-permute-done.14 = bf16[1024,256]{0,1:T(8,128)(2,1)S(1)} collective-permute-done((bf16[1024,256]{0,1:T(8,128)(2,1)}, bf16[1024,256]{0,1:T(8,128)(2,1)S(1)}, u32[]{:S(2)}, u32[]{:S(2)}) %collective-permute-start.14) | collective-permute-done | bytes 524320 | tf_op jit(solution)/shard_map/ppermute | solution.py:18
  590.7 10.5 %fusion.64 = f32[128,2,8,64]{3,2,1,0:T(8,128)} fusion(f32[128,2,64,64]{3,2,1,0:T(8,128)} %copy.552, f32[128,2,8,64]{3,0,2,1:T(8,128)S(1)} %copy-done.12), kind=kOutput, calls=%fused_computation.118 | convolution fusion | flops 100663296 | bytes 5242880 | tf_op jit(solution)/shard_map/bhtk,bhkv->bhtv/dot_general | solution.py:57
  669.6 18.4 %multiply_add_fusion.1 = f32[128,2,64,64]{3,2,1,0:T(8,128)} fusion(f32[128,2,64,64]{3,2,1,0:T(8,128)} %copy.495, f32[128,2]{1,0:T(8,128)S(1)} %bitcast.332, f32[128,2,8,64]{3,0,2,1:T(8,128)S(1)} %get-tuple-element.14, f32[128,2,8,64]{3,0,2,1:T(8,128)S(1)} %slice_subtract_fusion.1), kind=kOutput, calls=%fused_computation.15 | convolution fusion | flops 102760448 | bytes 9438208 | tf_op jit(solution)/shard_map/bhsk,bhsv->bhkv/dot_general | solution.py:62
  696.7 11.5 %convert_element_type.108 = f32[1024,4096]{0,1:T(8,128)} convert(bf16[1024,4096]{0,1:T(8,128)(2,1)} %copy-done) | non-fusion elementwise | flops 4194304 | bytes 25165824 | tf_op jit(solution)/shard_map/convert_element_type | solution.py:202
  709.1 18.4 %multiply_add_fusion = f32[128,2,64,64]{3,2,1,0:T(8,128)} fusion(f32[128,2,64,64]{3,2,1,0:T(8,128)} %copy.552, f32[128,2]{1,0:T(8,128)S(1)} %bitcast.333, f32[128,2,8,64]{3,0,2,1:T(8,128)S(1)} %copy-done.5, f32[128,2,8,64]{3,0,2,1:T(8,128)S(1)} %copy-done.7), kind=kOutput, calls=%fused_computation.14 | convolution fusion | flops 102760448 | bytes 9438208 | tf_op jit(solution)/shard_map/bhsk,bhsv->bhkv/dot_general | solution.py:62
  742.9 13.3 %copy.618 = f32[2,128,2,4096]{3,2,1,0:T(2,128)} copy(f32[2,128,2,4096]{1,3,2,0:T(8,128)} %pad_maximum_fusion) | data formatting | bytes 16777216
  759.8 29.5 %psum.7 = f32[1024]{0:T(1024)S(1)} all-reduce(f32[1024]{0:T(1024)S(1)} %fusion.8), channel_id=1, replica_groups=mesh['grp'=2,'tp'=16] {'tp'}, use_global_device_ids=true, to_apply=%region_12.13 | all-reduce | flops 1024 | bytes 8192 | tf_op jit(solution)/shard_map/psum | solution.py:149
  (513 shorter events, 406.8 us)
Async XLA Ops:
  7.2 80.6 %all-gather.4.cloned.1.call-start = ((), (), s32[]{:S(2)}) async-start(), calls=%async_computation | async-start | bytes 8912896 | tf_op jit(solution)/shard_map/all_gather | solution.py:197
  9.3 267.2 %all-gather.6.cloned.1.call-start = ((), (), s32[]{:S(2)}) async-start(), calls=%async_computation.1 | async-start | bytes 4456448 | tf_op jit(solution)/shard_map/all_gather | solution.py:139
  43.8 71.7 %copy-start.101 = (pred[8,8]{1,0:T(8,128)(4,1)}, pred[8,8]{1,0:T(8,128)(4,1)S(1)}, u32[]{:S(2)}) copy-start(pred[8,8]{1,0:T(8,128)(4,1)S(1)} %get-tuple-element.133) | copy-start | bytes 196
  43.8 71.7 %copy-start.102 = (pred[8,8]{1,0:T(8,128)(4,1)}, pred[8,8]{1,0:T(8,128)(4,1)S(1)}, u32[]{:S(2)}) copy-start(pred[8,8]{1,0:T(8,128)(4,1)S(1)} %get-tuple-element.132) | copy-start | bytes 196
  222.3 213.9 %copy-start.105 = (f32[128]{0:T(128)S(1)}, f32[128]{0:T(128)}, u32[]{:S(2)}) copy-start(f32[128]{0:T(128)} %get-tuple-element.12) | copy-start | bytes 1540
  222.3 214.5 %copy-start.51 = (f32[1,128,8,2]{1,3,2,0:T(2,128)S(1)}, f32[1,128,8,2]{1,3,2,0:T(2,128)}, u32[]{:S(2)}) copy-start(f32[1,128,8,2]{1,3,2,0:T(2,128)} %get-tuple-element.121) | copy-start | bytes 24580
  225.2 531.0 %all-gather.8.cloned.1.call-start = ((), (), s32[]{:S(2)}) async-start(), calls=%async_computation.2 | async-start | bytes 4456448 | tf_op jit(solution)/shard_map/all_gather | solution.py:139
  280.2 11.4 %collective-permute-start = (bf16[1024,256]{0,1:T(8,128)(2,1)S(1)}, bf16[1024,256]{0,1:T(8,128)(2,1)S(1)}, u32[]{:S(2)}, u32[]{:S(2)}) collective-permute-start(bf16[1024,256]{0,1:T(8,128)(2,1)S(1)} %convolution_convert_fusion.1), channel_id=1, source_target_pairs={{0,1},{1,2},{2,3},{3,4},{4,5},{5,6},{6,7},{7,8},{8,9},{9,10},{10,1... | collective-permute-start | bytes 1572872 | tf_op jit(solution)/shard_map/ppermute | solution.py:18
  291.6 11.3 %collective-permute-start.1 = (bf16[1024,256]{0,1:T(8,128)(2,1)S(1)}, bf16[1024,256]{0,1:T(8,128)(2,1)S(1)}, u32[]{:S(2)}, u32[]{:S(2)}) collective-permute-start(bf16[1024,256]{0,1:T(8,128)(2,1)S(1)} %collective-permute-done), channel_id=1, source_target_pairs={{0,1},{1,2},{2,3},{3,4},{4,5},{5,6},{6,7},{7,8},{8,9},{9,10},{10,1... | collective-permute-start | bytes 1572872 | tf_op jit(solution)/shard_map/ppermute | solution.py:18
  303.7 11.3 %collective-permute-start.2 = (bf16[1024,256]{0,1:T(8,128)(2,1)S(1)}, bf16[1024,256]{0,1:T(8,128)(2,1)S(1)}, u32[]{:S(2)}, u32[]{:S(2)}) collective-permute-start(bf16[1024,256]{0,1:T(8,128)(2,1)S(1)} %collective-permute-done.1), channel_id=1, source_target_pairs={{0,1},{1,2},{2,3},{3,4},{4,5},{5,6},{6,7},{7,8},{8,9},{9,10},{10,1... | collective-permute-start | bytes 1572872 | tf_op jit(solution)/shard_map/ppermute | solution.py:18
  315.8 11.3 %collective-permute-start.3 = (bf16[1024,256]{0,1:T(8,128)(2,1)S(1)}, bf16[1024,256]{0,1:T(8,128)(2,1)S(1)}, u32[]{:S(2)}, u32[]{:S(2)}) collective-permute-start(bf16[1024,256]{0,1:T(8,128)(2,1)S(1)} %collective-permute-done.2), channel_id=1, source_target_pairs={{0,1},{1,2},{2,3},{3,4},{4,5},{5,6},{6,7},{7,8},{8,9},{9,10},{10,1... | collective-permute-start | bytes 1572872 | tf_op jit(solution)/shard_map/ppermute | solution.py:18
  327.9 11.3 %collective-permute-start.4 = (bf16[1024,256]{0,1:T(8,128)(2,1)S(1)}, bf16[1024,256]{0,1:T(8,128)(2,1)S(1)}, u32[]{:S(2)}, u32[]{:S(2)}) collective-permute-start(bf16[1024,256]{0,1:T(8,128)(2,1)S(1)} %collective-permute-done.3), channel_id=1, source_target_pairs={{0,1},{1,2},{2,3},{3,4},{4,5},{5,6},{6,7},{7,8},{8,9},{9,10},{10,1... | collective-permute-start | bytes 1572872 | tf_op jit(solution)/shard_map/ppermute | solution.py:18
  340.0 11.3 %collective-permute-start.5 = (bf16[1024,256]{0,1:T(8,128)(2,1)S(1)}, bf16[1024,256]{0,1:T(8,128)(2,1)S(1)}, u32[]{:S(2)}, u32[]{:S(2)}) collective-permute-start(bf16[1024,256]{0,1:T(8,128)(2,1)S(1)} %collective-permute-done.4), channel_id=1, source_target_pairs={{0,1},{1,2},{2,3},{3,4},{4,5},{5,6},{6,7},{7,8},{8,9},{9,10},{10,1... | collective-permute-start | bytes 1572872 | tf_op jit(solution)/shard_map/ppermute | solution.py:18
  352.1 11.3 %collective-permute-start.6 = (bf16[1024,256]{0,1:T(8,128)(2,1)S(1)}, bf16[1024,256]{0,1:T(8,128)(2,1)S(1)}, u32[]{:S(2)}, u32[]{:S(2)}) collective-permute-start(bf16[1024,256]{0,1:T(8,128)(2,1)S(1)} %collective-permute-done.5), channel_id=1, source_target_pairs={{0,1},{1,2},{2,3},{3,4},{4,5},{5,6},{6,7},{7,8},{8,9},{9,10},{10,1... | collective-permute-start | bytes 1572872 | tf_op jit(solution)/shard_map/ppermute | solution.py:18
  364.2 11.3 %collective-permute-start.7 = (bf16[1024,256]{0,1:T(8,128)(2,1)S(1)}, bf16[1024,256]{0,1:T(8,128)(2,1)S(1)}, u32[]{:S(2)}, u32[]{:S(2)}) collective-permute-start(bf16[1024,256]{0,1:T(8,128)(2,1)S(1)} %collective-permute-done.6), channel_id=1, source_target_pairs={{0,1},{1,2},{2,3},{3,4},{4,5},{5,6},{6,7},{7,8},{8,9},{9,10},{10,1... | collective-permute-start | bytes 1572872 | tf_op jit(solution)/shard_map/ppermute | solution.py:18
  376.3 11.3 %collective-permute-start.8 = (bf16[1024,256]{0,1:T(8,128)(2,1)S(1)}, bf16[1024,256]{0,1:T(8,128)(2,1)S(1)}, u32[]{:S(2)}, u32[]{:S(2)}) collective-permute-start(bf16[1024,256]{0,1:T(8,128)(2,1)S(1)} %collective-permute-done.7), channel_id=1, source_target_pairs={{0,1},{1,2},{2,3},{3,4},{4,5},{5,6},{6,7},{7,8},{8,9},{9,10},{10,1... | collective-permute-start | bytes 1572872 | tf_op jit(solution)/shard_map/ppermute | solution.py:18
  388.4 11.3 %collective-permute-start.9 = (bf16[1024,256]{0,1:T(8,128)(2,1)S(1)}, bf16[1024,256]{0,1:T(8,128)(2,1)S(1)}, u32[]{:S(2)}, u32[]{:S(2)}) collective-permute-start(bf16[1024,256]{0,1:T(8,128)(2,1)S(1)} %collective-permute-done.8), channel_id=1, source_target_pairs={{0,1},{1,2},{2,3},{3,4},{4,5},{5,6},{6,7},{7,8},{8,9},{9,10},{10,1... | collective-permute-start | bytes 1572872 | tf_op jit(solution)/shard_map/ppermute | solution.py:18
  400.5 11.3 %collective-permute-start.10 = (bf16[1024,256]{0,1:T(8,128)(2,1)S(1)}, bf16[1024,256]{0,1:T(8,128)(2,1)S(1)}, u32[]{:S(2)}, u32[]{:S(2)}) collective-permute-start(bf16[1024,256]{0,1:T(8,128)(2,1)S(1)} %collective-permute-done.9), channel_id=1, source_target_pairs={{0,1},{1,2},{2,3},{3,4},{4,5},{5,6},{6,7},{7,8},{8,9},{9,10},{10,1... | collective-permute-start | bytes 1572872 | tf_op jit(solution)/shard_map/ppermute | solution.py:18
  412.6 11.3 %collective-permute-start.11 = (bf16[1024,256]{0,1:T(8,128)(2,1)S(1)}, bf16[1024,256]{0,1:T(8,128)(2,1)S(1)}, u32[]{:S(2)}, u32[]{:S(2)}) collective-permute-start(bf16[1024,256]{0,1:T(8,128)(2,1)S(1)} %collective-permute-done.10), channel_id=1, source_target_pairs={{0,1},{1,2},{2,3},{3,4},{4,5},{5,6},{6,7},{7,8},{8,9},{9,10},{10,1... | collective-permute-start | bytes 1572872 | tf_op jit(solution)/shard_map/ppermute | solution.py:18
  424.7 11.4 %collective-permute-start.12 = (bf16[1024,256]{0,1:T(8,128)(2,1)S(1)}, bf16[1024,256]{0,1:T(8,128)(2,1)}, u32[]{:S(2)}, u32[]{:S(2)}) collective-permute-start(bf16[1024,256]{0,1:T(8,128)(2,1)S(1)} %collective-permute-done.11), channel_id=1, source_target_pairs={{0,1},{1,2},{2,3},{3,4},{4,5},{5,6},{6,7},{7,8},{8,9},{9,10},{10,1... | collective-permute-start | bytes 1572872 | tf_op jit(solution)/shard_map/ppermute | solution.py:18
  436.2 17.2 %collective-permute-start.13 = (bf16[1024,256]{0,1:T(8,128)(2,1)}, bf16[1024,256]{0,1:T(8,128)(2,1)}, u32[]{:S(2)}, u32[]{:S(2)}) collective-permute-start(bf16[1024,256]{0,1:T(8,128)(2,1)} %collective-permute-done.12), channel_id=1, source_target_pairs={{0,1},{1,2},{2,3},{3,4},{4,5},{5,6},{6,7},{7,8},{8,9},{9,10},{10,1... | collective-permute-start | bytes 1572872 | tf_op jit(solution)/shard_map/ppermute | solution.py:18
  453.4 29.3 %copy-start.18 = (bf16[1024,256]{0,1:T(8,128)(2,1)S(1)}, bf16[1024,256]{0,1:T(8,128)(2,1)}, u32[]{:S(2)}) copy-start(bf16[1024,256]{0,1:T(8,128)(2,1)} %copy-done.17) | copy-start | bytes 1572868
  453.4 30.2 %copy-start.16 = (bf16[1024,256]{0,1:T(8,128)(2,1)S(1)}, bf16[1024,256]{0,1:T(8,128)(2,1)}, u32[]{:S(2)}) copy-start(bf16[1024,256]{0,1:T(8,128)(2,1)} %copy-done.15) | copy-start | bytes 1572868
  453.4 11.6 %collective-permute-start.14 = (bf16[1024,256]{0,1:T(8,128)(2,1)}, bf16[1024,256]{0,1:T(8,128)(2,1)S(1)}, u32[]{:S(2)}, u32[]{:S(2)}) collective-permute-start(bf16[1024,256]{0,1:T(8,128)(2,1)} %collective-permute-done.13), channel_id=1, source_target_pairs={{0,1},{1,2},{2,3},{3,4},{4,5},{5,6},{6,7},{7,8},{8,9},{9,10},{10,1... | collective-permute-start | bytes 1572872 | tf_op jit(solution)/shard_map/ppermute | solution.py:18
  (116 other events, 793.8 us)
Sparse Core Ops, SparseCore 0:
  10.7 77.0 all-gather.3
  225.4 51.0 all-gather.5
  668.2 49.7 all-gather.7
